TPU v7x, 128 devices: a whole 4x4x4 slice. The times are simulated.
128 devices in a mesh: ep: 64 (over z, y, x), tp: 2 (over core).
Axes of the slice: x: 4, y: 4, z: 4, core: 2. Of those that a mesh axis runs over, the one named last changes fastest.
Arguments:
- tokens: bfloat16 [1024, 2048], P('ep'), may hold values from -6 to 6
- norm_gain: float32 [2048], replicated, may hold values from 0.1 to 1.9
- query_weight: bfloat16 [2048, 1024], P('ep', 'tp'), may hold values from -0.125 to 0.125
- key_weight: bfloat16 [2048, 1024], P('ep', 'tp'), may hold values from -0.125 to 0.125
- value_weight: bfloat16 [2048, 1024], P('ep', 'tp'), may hold values from -0.125 to 0.125
- outgate_weight: bfloat16 [2048, 1024], P('ep', 'tp'), may hold values from -0.125 to 0.125
- input_weight: bfloat16 [2048, 8], P('ep', 'tp'), may hold values from -0.125 to 0.125
- forget_weight: bfloat16 [2048, 8], P('ep', 'tp'), may hold values from -0.125 to 0.125
- forget_bias: float32 [8], P('tp'), may hold values from -1 to 5
- memory: float32 [1024, 8, 128, 128], P('ep', 'tp'), may hold values from -2.4 to 2.4
- stabilizer: float32 [1024, 8], P('ep', 'tp'), may hold values from -3 to 3
- head_gain: float32 [1024], P('tp'), may hold values from 0.1 to 1.9
- mix_weight: bfloat16 [1024, 2048], P('tp', 'ep'), may hold values from -0.1875 to 0.1875
- second_gain: float32 [2048], replicated, may hold values from 0.1 to 1.9
- route_experts: int32 [1024, 4], P('ep'), may hold values from 0 to 63, all different within a row; in each aligned block of 16 rows (0 to 15, 16 to 31, ...) at most 2 rows name the same one
- route_weight: float32 [1024, 4], P('ep'), may hold values from 0.1 to 1
- expert_gate: bfloat16 [64, 2048, 2048], P('ep', None, 'tp'), may hold values from -0.5 to 0.5
- expert_up: bfloat16 [64, 2048, 2048], P('ep', None, 'tp'), may hold values from -0.5 to 0.5
- expert_down: bfloat16 [64, 2048, 2048], P('ep', 'tp'), may hold values from -0.03125 to 0.03125
- dense_gate: bfloat16 [4096, 2048], P(('ep', 'tp')), may hold values from -0.125 to 0.125
- dense_up: bfloat16 [4096, 2048], P(('ep', 'tp')), may hold values from -0.125 to 0.125
- dense_down: bfloat16 [4096, 2048], P(('ep', 'tp')), may hold values from -0.09375 to 0.09375
- branch_scale: float32 [2048], replicated, may hold values from 0.3 to 1.5
Outputs:
- mixed: bfloat16 [1024, 2048], P('ep', 'tp')
- memory_new: float32 [1024, 8, 128, 128], P('ep', 'tp')
- stabilizer_new: float32 [1024, 8], P('ep', 'tp')
Inputs may be any that keep to these rules, and one draw needn't show every extreme that they name: `route_experts`: each row names 4 different experts. Within each aligned block of 16 rows no expert is named by more than 2 rows, and in every draw some expert is named by exactly 2 rows of some block.
All inputs are finite; a program needn't handle non-finite values.
Results may differ from a plain program's by a relative error of at most 0.03.
Values may be sent and summed in bfloat16 or wider, within the bound.
A program may use at most 128 MiB of HBM per device.

v0:
```python
import jax
import jax.numpy as jnp
from jax import lax
from jax.sharding import PartitionSpec as P

norm_eps = 1e-05
clamp_limit = 7.0
sigmoid_slope = 1.702


def in_one_piece(arrays, axis, dim, along):
    widths = [a.shape[along] for a in arrays]
    both = jnp.concatenate(arrays, axis=along)
    whole = lax.all_gather(both, axis, axis=dim, tiled=True)
    return tuple(jnp.split(whole, [sum(widths[:k]) for k in range(1, len(widths))], axis=along))


def sent_to_all(shard, axis):
    devices = lax.axis_size(axis)
    return lax.all_to_all(
        jnp.broadcast_to(shard[None], (devices, *shard.shape)), axis, 0, 0, tiled=True
    )


def taken_together(shard, axis):
    return sent_to_all(shard, axis).astype(jnp.float32).sum(axis=0)


def cut_along(shard, dim, devices):
    lengths = shard.shape
    pieces = shard.reshape(*lengths[:dim], devices, lengths[dim] // devices, *lengths[dim + 1 :])
    return jnp.moveaxis(pieces, dim, 0)


def sent_and_summed(shard, axis, dim):
    devices = lax.axis_size(axis)
    pieces = lax.all_to_all(cut_along(shard, dim, devices), axis, 0, 0, tiled=True)
    return jnp.sum(pieces.astype(jnp.float32), axis=0)


def rms_scale(values, gain):
    mean_square = jnp.mean(values * values, axis=-1, keepdims=True)
    return values * lax.rsqrt(mean_square + norm_eps) * gain


def round_half(values):
    return lax.optimization_barrier(values.astype(jnp.bfloat16)).astype(jnp.float32)


def clamped_unit(gate_pre, up_pre):
    gate_clamped = jnp.minimum(gate_pre, clamp_limit)
    up_clamped = jnp.clip(up_pre, -clamp_limit, clamp_limit)
    return (
        (up_clamped + 1.0) * gate_clamped * jax.nn.sigmoid(sigmoid_slope * gate_clamped)
    ).astype(jnp.bfloat16)


def memory_step(projected, forget_bias, memory, stabilizer, head_gain):
    query_rows, key_rows, value_rows, outgate_rows, input_pre, forget_pre = projected
    sequences, head_count = stabilizer.shape
    head_size = memory.shape[-1]
    log_forget = jax.nn.log_sigmoid(forget_pre + forget_bias)
    stab_new = jnp.maximum(log_forget + stabilizer, input_pre)
    carried = jnp.exp(log_forget + stabilizer - stab_new)
    written = jnp.exp(input_pre - stab_new)
    query_heads = query_rows.astype(jnp.float32).reshape(sequences, head_count, head_size)
    key_heads = key_rows.astype(jnp.float32).reshape(
        sequences, head_count, head_size
    ) * head_size ** (-0.5)
    value_heads = value_rows.astype(jnp.float32).reshape(sequences, head_count, head_size)
    memory_new = (
        carried[:, :, None, None] * memory
        + written[:, :, None, None] * value_heads[:, :, :, None] * key_heads[:, :, None, :]
    )
    readout = jnp.einsum("bhvk,bhk->bhv", memory_new, query_heads)
    out_gate = jax.nn.sigmoid(
        outgate_rows.astype(jnp.float32).reshape(sequences, head_count, head_size)
    )
    gated = (rms_scale(readout, head_gain.reshape(head_count, head_size)) * out_gate).astype(
        jnp.bfloat16
    )
    return (gated.reshape(sequences, head_count * head_size), memory_new, stab_new)


def expert_apply(rows, gate_weight, up_weight, down_weight):
    gate_pre = jnp.dot(rows, gate_weight, preferred_element_type=jnp.float32)
    up_pre = jnp.dot(rows, up_weight, preferred_element_type=jnp.float32)
    activity = clamped_unit(gate_pre, up_pre)
    return jnp.dot(activity, down_weight, preferred_element_type=jnp.float32).astype(jnp.bfloat16)


def slot_table(hit_mask, capacity):
    ranks = jnp.cumsum(hit_mask, axis=1) - 1.0
    slots = jnp.arange(capacity).astype(jnp.float32)
    return hit_mask[:, None, :] * (ranks[:, None, :] == slots[None, :, None]).astype(jnp.float32)


def body(
    tokens,
    norm_gain,
    query_weight,
    key_weight,
    value_weight,
    outgate_weight,
    input_weight,
    forget_weight,
    forget_bias,
    memory,
    stabilizer,
    head_gain,
    mix_weight,
    second_gain,
    route_experts,
    route_weight,
    expert_gate,
    expert_up,
    expert_down,
    dense_gate,
    dense_up,
    dense_down,
    branch_scale,
):
    sequences, model_width = tokens.shape
    ep_count = lax.axis_size("ep")
    tp_count = lax.axis_size("tp")
    part_width = model_width // tp_count
    top_count = route_experts.shape[1]
    expert_count = expert_gate.shape[0] * ep_count
    capacity = max(2, 2 * sequences * top_count // expert_count)
    inputs_float = tokens.astype(jnp.float32)
    normed = rms_scale(inputs_float, norm_gain).astype(jnp.bfloat16)
    pieces = in_one_piece(
        (query_weight, key_weight, value_weight, outgate_weight, input_weight, forget_weight),
        "ep",
        0,
        1,
    )
    sums = tuple((jnp.dot(normed, piece, preferred_element_type=jnp.float32) for piece in pieces))
    projected = (
        sums[0].astype(jnp.bfloat16),
        sums[1].astype(jnp.bfloat16),
        sums[2].astype(jnp.bfloat16),
        sums[3].astype(jnp.bfloat16),
        sums[4],
        sums[5],
    )
    gated, memory_new, stab_new = memory_step(projected, forget_bias, memory, stabilizer, head_gain)
    partial_value = jnp.dot(
        gated,
        lax.all_gather(mix_weight, "ep", axis=1, tiled=True),
        preferred_element_type=jnp.float32,
    )
    attended = taken_together(round_half(partial_value).astype(jnp.bfloat16), "tp").astype(
        jnp.float32
    )
    residual = (inputs_float + attended).astype(jnp.bfloat16)
    residual_float = residual.astype(jnp.float32)
    normed_second = rms_scale(residual_float, second_gain).astype(jnp.bfloat16)
    own_residual = lax.dynamic_slice_in_dim(
        residual_float, lax.axis_index("tp") * part_width, part_width, 1
    )
    own_scale = lax.dynamic_slice_in_dim(
        branch_scale, lax.axis_index("tp") * part_width, part_width, 0
    )
    matched = route_experts[:, :, None] == jnp.arange(expert_count)[None, None, :]
    hit_mask = jnp.any(matched, axis=1).astype(jnp.float32).T
    weights = jnp.sum(jnp.where(matched, route_weight[:, :, None], 0.0), axis=1).T
    select = slot_table(hit_mask, capacity)
    outgoing = jnp.einsum(
        "ecs,sd->ecd",
        select.astype(jnp.bfloat16),
        normed_second,
        preferred_element_type=jnp.float32,
    ).astype(jnp.bfloat16)
    received = lax.all_to_all(outgoing, "ep", split_axis=0, concat_axis=0, tiled=True)
    count = received.shape[1]
    partial_out = expert_apply(
        received.reshape(-1, model_width), expert_gate[0], expert_up[0], expert_down[0]
    )
    halves = sent_and_summed(partial_out.astype(jnp.float32).astype(jnp.bfloat16), "tp", 1)
    returned = lax.all_to_all(
        halves.reshape(ep_count, count, part_width).astype(jnp.bfloat16),
        "ep",
        split_axis=0,
        concat_axis=0,
        tiled=True,
    ).astype(jnp.float32)
    routed = jnp.einsum("ecs,ecd->sd", select * weights[:, None, :], returned)
    gate_piece, up_piece, down_piece = in_one_piece((dense_gate, dense_up, dense_down), "ep", 0, 1)
    gate_rows = jnp.einsum(
        "td,fd->tf", normed_second, gate_piece, preferred_element_type=jnp.float32
    )
    lift_rows = jnp.einsum("td,fd->tf", normed_second, up_piece, preferred_element_type=jnp.float32)
    activity = (jax.nn.silu(gate_rows) * lift_rows).astype(jnp.bfloat16)
    total = jnp.dot(activity, down_piece, preferred_element_type=jnp.float32)
    halves = sent_and_summed(total.astype(jnp.bfloat16), "tp", 1)
    branch = halves * own_scale
    mixed = own_residual + routed + branch
    return (mixed.astype(jnp.bfloat16), memory_new, stab_new)


def solution(mesh):
    in_specs = (
        P("ep", None),
        P(),
        P("ep", "tp"),
        P("ep", "tp"),
        P("ep", "tp"),
        P("ep", "tp"),
        P("ep", "tp"),
        P("ep", "tp"),
        P("tp"),
        P("ep", "tp", None, None),
        P("ep", "tp"),
        P("tp"),
        P("tp", "ep"),
        P(),
        P("ep", None),
        P("ep", None),
        P("ep", None, "tp"),
        P("ep", None, "tp"),
        P("ep", "tp", None),
        P(("ep", "tp"), None),
        P(("ep", "tp"), None),
        P(("ep", "tp"), None),
        P(),
    )
    out_specs = (P("ep", "tp"), P("ep", "tp", None, None), P("ep", "tp"))
    return jax.shard_map(body, mesh=mesh, in_specs=in_specs, out_specs=out_specs, check_vma=False)
```

profile of v0, /device:TPU:0, one launch (start us, length us, event | category | flops | bytes accessed | tf_op | source)
XLA Modules:
  0.0 342.2 jit_solution(8388457338373234706)
XLA Ops:
  7.2 0.8 copy.56
  8.0 0.8 copy.57
  8.8 1.5 concatenate.6
  10.4 0.0 all-gather.6.cloned.1.call-start
  10.4 0.7 all-gather.6.cloned.1.call-update
  11.2 1.8 pad_maximum_fusion
  13.0 0.8 fusion.119
  13.8 0.1 copy.60
  13.9 0.2 reduce_window_sum.11
  14.1 0.1 copy.61
  14.1 1.0 fusion.107
  15.1 78.9 %all-gather.4.cloned.1.call-done = bf16[2048,2056]{1,0:T(8,128)(2,1)} async-done(((bf16[32,2056]{1,0:T(8,128)(2,1)}), bf16[2048,2056]{1,0:T(8,128)(2,1)}) %all-gather.4.cloned.1.call-update) | async-done | bytes 8421392 | tf_op jit(solution)/shard_map/all_gather | solution.py:14
  94.0 1.3 fusion.94
  95.3 1.8 subtract_exponential_fusion.1
  97.1 0.1 copy.59
  97.2 2.1 fusion.58
  99.3 0.1 copy.58
  99.4 2.0 fusion.67
  101.4 2.0 fusion.70
  103.4 2.0 fusion.88
  105.5 0.1 broadcast_multiply_fusion
  105.6 3.1 multiply_add_fusion
  108.7 2.0 copy-done
  110.7 1.2 fusion.149
  111.8 0.1 multiply_reduce_fusion.1
  112.0 0.1 multiply_convert_fusion.1
  112.1 49.8 %all-gather.6.cloned.1.call-done = bf16[512,2048]{0,1:T(8,128)(2,1)} async-done(((bf16[512,32]{0,1:T(8,128)(2,1)}), bf16[512,2048]{0,1:T(8,128)(2,1)}) %all-gather.6.cloned.1.call-update) | async-done | bytes 2097168 | tf_op jit(solution)/shard_map/all_gather | solution.py:150
  161.8 2.2 convolution_convert_fusion.1
  164.1 3.8 %all_to_all.25 = bf16[2,16,2048]{2,1,0:T(8,128)(2,1)S(1)} all-to-all(bf16[2,16,2048]{2,1,0:T(8,128)(2,1)S(1)} %broadcast_in_dim.10), channel_id=1, replica_groups=mesh['ep'=64,'tp'=2] {'tp'}, dimensions={0} | all-to-all | bytes 262144 | tf_op jit(solution)/shard_map/all_to_all | solution.py:20
  168.0 0.1 multiply_reduce_fusion
  168.1 0.1 multiply_convert_fusion
  168.2 0.4 convolution_convert_fusion
  168.6 0.5 copy.62
  169.2 22.5 %all_to_all.26 = bf16[64,2,2048]{2,1,0:T(2,128)(2,1)S(1)} all-to-all(bf16[64,2,2048]{2,1,0:T(2,128)(2,1)S(1)} %copy.62), channel_id=1, replica_groups=mesh['ep'=64,'tp'=2] {'ep'}, dimensions={0} | all-to-all | bytes 1048576 | tf_op jit(solution)/shard_map/all_to_all | solution.py:175
  191.7 0.2 reshape.97
  191.9 2.9 fusion.37
  194.8 5.5 %fusion.12 = bf16[128,2048]{1,0:T(8,128)(2,1)S(1)} fusion(bf16[1,1024,2048]{2,1,0:T(8,128)(2,1)} %param.41, f32[128,1024]{1,0:T(8,128)S(1)} %fusion.37, bf16[128,2048]{1,0:T(8,128)(2,1)S(1)} %reshape.97, bf16[1,2048,1024]{2,1,0:T(8,128)(2,1)} %param.40), kind=kOutput, calls=%fused_computation.13 | convolution fusion | flops 1075183616 | bytes 9961472 | tf_op jit(solution)/shard_map/dot_general | solution.py:89
  200.4 4.2 %all_to_all.27 = bf16[2,128,1024]{2,1,0:T(8,128)(2,1)S(1)} all-to-all(bf16[2,128,1024]{2,1,0:T(8,128)(2,1)S(1)} %bitcast.67), channel_id=1, replica_groups=mesh['ep'=64,'tp'=2] {'tp'}, dimensions={0} | all-to-all | bytes 1048576 | tf_op jit(solution)/shard_map/all_to_all | solution.py:37
  204.5 0.1 reduce_sum.71
  204.6 0.8 convert_element_type.114
  205.4 91.2 %all-gather.8.cloned.1.call-done = bf16[2048,6144]{1,0:T(8,128)(2,1)} async-done(((bf16[32,6144]{1,0:T(8,128)(2,1)}), bf16[2048,6144]{1,0:T(8,128)(2,1)}) %all-gather.8.cloned.1.call-update) | async-done | bytes 25165840 | tf_op jit(solution)/shard_map/all_gather | solution.py:14
  296.6 5.6 %fusion.4 = f32[16,2048]{1,0:T(8,128)S(1)} fusion(bf16[16,2048]{1,0:T(8,128)(2,1)S(1)} %multiply_convert_fusion, bf16[2048,6144]{1,0:T(8,128)(2,1)} %all-gather.8.cloned.1.call-done), kind=kOutput, calls=%fused_computation.4 | convolution fusion | flops 134217728 | bytes 8585216 | tf_op jit(solution)/shard_map/td,fd->tf/dot_general | solution.py:190
  302.3 9.2 %fusion.21 = bf16[16,2048]{1,0:T(8,128)(2,1)S(1)} fusion(bf16[2048,6144]{1,0:T(8,128)(2,1)} %all-gather.8.cloned.1.call-done, bf16[16,2048]{1,0:T(8,128)(2,1)S(1)} %multiply_convert_fusion, f32[16,2048]{1,0:T(8,128)S(1)} %fusion.4), kind=kOutput, calls=%fused_computation.17 | convolution fusion | flops 268664832 | bytes 17039360 | tf_op jit(solution)/shard_map/dot_general | solution.py:195
  311.5 3.8 %all_to_all.28 = bf16[2,16,1024]{2,1,0:T(8,128)(2,1)S(1)} all-to-all(bf16[2,16,1024]{2,1,0:T(8,128)(2,1)S(1)} %bitcast.71), channel_id=1, replica_groups=mesh['ep'=64,'tp'=2] {'tp'}, dimensions={0} | all-to-all | bytes 131072 | tf_op jit(solution)/shard_map/all_to_all | solution.py:37
  315.2 8.6 %all-to-all-start.3 = ((bf16[64,2,1024]{2,1,0:T(2,128)(2,1)}), bf16[64,2,1024]{2,1,0:T(2,128)(2,1)S(1)}, u32[]{:S(2)}, u32[]{:S(2)}) async-start(bf16[64,2,1024]{2,1,0:T(2,128)(2,1)} %convert_element_type.114), calls=%async_computation.3 | async-start | bytes 524288 | tf_op jit(solution)/shard_map/all_to_all | solution.py:181
  323.9 0.1 select_reduce_fusion
  324.0 10.8 %all-to-all-done.3 = bf16[64,2,1024]{2,1,0:T(2,128)(2,1)S(1)} async-done(((bf16[64,2,1024]{2,1,0:T(2,128)(2,1)}), bf16[64,2,1024]{2,1,0:T(2,128)(2,1)S(1)}, u32[]{:S(2)}, u32[]{:S(2)}) %all-to-all-start.3) | async-done | bytes 262176 | tf_op jit(solution)/shard_map/all_to_all | solution.py:181
  334.8 0.9 fusion.54
  (38 shorter events, 0.4 us)
Async XLA Ops:
  7.2 92.2 %copy-start.1 = (bf16[16,2048]{1,0:T(8,128)(2,1)S(1)}, bf16[16,2048]{1,0:T(8,128)(2,1)}, u32[]{:S(2)}) copy-start(bf16[16,2048]{1,0:T(8,128)(2,1)} %param.23) | copy-start | bytes 196612
  7.2 92.2 %copy-start.8 = (f32[2048]{0:T(1024)S(1)}, f32[2048]{0:T(1024)}, u32[]{:S(2)}) copy-start(f32[2048]{0:T(1024)} %param.24) | copy-start | bytes 24580
  7.2 86.8 %all-gather.4.cloned.1.call-start = ((), (), s32[]{:S(2)}) async-start(), calls=%async_computation.5 | async-start | bytes 9052160 | tf_op jit(solution)/shard_map/all_gather | solution.py:14
  10.4 151.5 %all-gather.6.cloned.1.call-start = ((), (), s32[]{:S(2)}) async-start(), calls=%async_computation.6 | async-start | bytes 2129920 | tf_op jit(solution)/shard_map/all_gather | solution.py:150
  11.1 285.5 %all-gather.8.cloned.1.call-start = ((), (), s32[]{:S(2)}) async-start(), calls=%async_computation.7 | async-start | bytes 25559040 | tf_op jit(solution)/shard_map/all_gather | solution.py:14
  97.1 8.4 %copy-start.5 = (f32[16,4]{0,1:T(4,128)}, f32[16,4]{0,1:T(4,128)S(1)}, u32[]{:S(2)}) copy-start(f32[16,4]{0,1:T(4,128)S(1)} %get-tuple-element.6) | copy-start | bytes 772
  108.7 2.0 copy-start
  110.7 1.3 copy-start.4
  110.7 57.5 %copy-start.2 = (f32[2048]{0:T(1024)S(1)}, f32[2048]{0:T(1024)}, u32[]{:S(2)}) copy-start(f32[2048]{0:T(1024)} %param.36) | copy-start | bytes 24580
  302.2 21.6 %copy-start.6 = (f32[2048]{0:T(1024)S(1)}, f32[2048]{0:T(1024)}, u32[]{:S(2)}) copy-start(f32[2048]{0:T(1024)} %param.45) | copy-start | bytes 24580
  302.2 21.7 %copy-start.3 = (s32[16,4]{0,1:T(4,128)S(1)}, s32[16,4]{0,1:T(4,128)}, u32[]{:S(2)}) copy-start(s32[16,4]{0,1:T(4,128)} %param.37) | copy-start | bytes 772
  302.2 21.7 %copy-start.7 = (f32[16,4]{0,1:T(4,128)S(1)}, f32[16,4]{0,1:T(4,128)}, u32[]{:S(2)}) copy-start(f32[16,4]{0,1:T(4,128)} %param.38) | copy-start | bytes 772
  315.2 19.5 %all-to-all-start.3 = ((bf16[64,2,1024]{2,1,0:T(2,128)(2,1)}), bf16[64,2,1024]{2,1,0:T(2,128)(2,1)S(1)}, u32[]{:S(2)}, u32[]{:S(2)}) async-start(bf16[64,2,1024]{2,1,0:T(2,128)(2,1)} %convert_element_type.114), calls=%async_computation.3 | async-start | bytes 524288 | tf_op jit(solution)/shard_map/all_to_all | solution.py:181
Sparse Core Ops, SparseCore 0:
  11.3 82.5 all-gather.3
  96.8 64.9 all-gather.5
  164.6 131.9 all-gather.7
where the time goes:
time: 343 us; the launch traced here: 342 us
  waiting for transfers between devices  231 us (67%)
  matrix products  39.2 us (11%)
  blocking collectives  34.3 us (10%)
  between operations  14 us (4%)
  starting transfers between devices  8.72 us (3%)
  other arithmetic  7.55 us (2%)
  local copies, waits for them, and re-layouts  7.16 us (2%)
    all_gather x2, waiting for transfers between devices, in_one_piece(): whole = lax.all_gather(both, axis, axis=dim, tiled=True)  170 us
    all_gather x1, waiting for transfers between devices, body(): lax.all_gather(mix_weight, 'ep', axis=1, tiled=True)  49.8 us
    all_to_all x1, blocking collectives, body(): lax.all_to_all(outgoing, 'ep', split_axis=0, concat_axis=0, tiled=True)  22.5 us
    dot_general x6, matrix products, body(): jnp.dot(normed, piece, preferred_element_type=jnp.float32)  11.2 us
    all_to_all x1, waiting for transfers between devices, body(): lax.all_to_all(halves.reshape(ep_count, count, part_width).astype(jnp.bfl...  10.8 us
    dot_general x1, matrix products, body(): total = jnp.dot(activity, down_piece, preferred_element_type=jnp.float32)  9.18 us
    all_to_all x1, starting transfers between devices, body(): lax.all_to_all(halves.reshape(ep_count, count, part_width).astype(jnp.bfl...  8.6 us
    all_to_all x2, blocking collectives, sent_and_summed(): lax.all_to_all(cut_along(shard, dim, devices), axis, 0, 0, tiled=True)  7.95 us
  transfers between devices with their start and end apart: 4, of which 4 were waited for; matrix products, arithmetic and copies ran while one was open for 10% of the time, Pallas kernels for 0%

commit v1 on v0

--- a/solution.py
+++ b/solution.py
@@ -6,6 +6,13 @@
 norm_eps = 1e-05
 clamp_limit = 7.0
 sigmoid_slope = 1.702
+
+
+def gather_over(block, axis, along):
+    size = lax.axis_size(axis)
+    parts = jnp.stack([block for _ in range(size)])
+    parts = lax.all_to_all(parts, axis, split_axis=0, concat_axis=0)
+    return jnp.concatenate(parts, axis=along)
 
 
 def in_one_piece(arrays, axis, dim, along):
@@ -146,9 +153,7 @@
     )
     gated, memory_new, stab_new = memory_step(projected, forget_bias, memory, stabilizer, head_gain)
     partial_value = jnp.dot(
-        gated,
-        lax.all_gather(mix_weight, "ep", axis=1, tiled=True),
-        preferred_element_type=jnp.float32,
+        gated, gather_over(mix_weight, "ep", 1), preferred_element_type=jnp.float32
     )
     attended = taken_together(round_half(partial_value).astype(jnp.bfloat16), "tp").astype(
         jnp.float32

time: 343 us -> 295 us (0.86)
  waiting for transfers between devices: 231 us -> 169 us
  starting transfers between devices: 8.72 us -> 20.2 us
  blocking collectives: 34.3 us -> 38.1 us
    all_gather x1 -> x0, waiting for transfers between devices: 49.8 us -> none  [body(): lax.all_gather(mix_weight, 'ep', axis=1, tiled=True)]
    all_gather x2, waiting for transfers between devices: 170 us -> 158 us  [in_one_piece(): whole = lax.all_gather(both, axis, axis=dim, tiled=True)]
    all_to_all x0 -> x1, starting transfers between devices: none -> 11.5 us  [gather_over(): parts = lax.all_to_all(parts, axis, split_axis=0, concat_axis=0)]
    all_to_all x1, blocking collectives: 22.5 us -> 26.4 us  [body(): lax.all_to_all(outgoing, 'ep', split_axis=0, concat_axis=0, tiled=True)]
  transfers between devices with their start and end apart: 4 -> 4, of which waited for: 4 -> 3; matrix products, arithmetic and copies ran while one was open for 10% -> 11% of each run, Pallas kernels for 0% -> 0%
where the time goes in v1:
time: 295 us; the launch traced here: 294 us
  waiting for transfers between devices  169 us (57%)
  blocking collectives  38.1 us (13%)
  matrix products  37 us (13%)
  starting transfers between devices  20.2 us (7%)
  between operations  14.4 us (5%)
  local copies, waits for them, and re-layouts  9.45 us (3%)
  other arithmetic  6.15 us (2%)
    all_gather x2, waiting for transfers between devices, in_one_piece(): whole = lax.all_gather(both, axis, axis=dim, tiled=True)  158 us
    all_to_all x1, blocking collectives, body(): lax.all_to_all(outgoing, 'ep', split_axis=0, concat_axis=0, tiled=True)  26.4 us
    all_to_all x1, starting transfers between devices, gather_over(): parts = lax.all_to_all(parts, axis, split_axis=0, concat_axis=0)  11.5 us
    dot_general x6, matrix products, body(): jnp.dot(normed, piece, preferred_element_type=jnp.float32)  11 us
    all_to_all x1, waiting for transfers between devices, body(): lax.all_to_all(halves.reshape(ep_count, count, part_width).astype(jnp.bfl...  10.8 us
    dot_general x1, matrix products, body(): total = jnp.dot(activity, down_piece, preferred_element_type=jnp.float32)  9.19 us
    all_to_all x1, starting transfers between devices, body(): lax.all_to_all(halves.reshape(ep_count, count, part_width).astype(jnp.bfl...  8.6 us
    all_to_all x2, blocking collectives, sent_and_summed(): lax.all_to_all(cut_along(shard, dim, devices), axis, 0, 0, tiled=True)  7.95 us
  transfers between devices with their start and end apart: 4, of which 3 were waited for; matrix products, arithmetic and copies ran while one was open for 11% of the time, Pallas kernels for 0%

profile of v1, /device:TPU:0, one launch (start us, length us, event | category | flops | bytes accessed | tf_op | source)
XLA Modules:
  0.0 294.3 jit_solution(6559463762706027675)
XLA Ops:
  7.2 0.8 copy.57
  8.0 0.8 copy.58
  8.8 1.5 concatenate.6
  10.4 0.0 all-gather.5.cloned.1.call-start
  10.4 1.8 pad_maximum_fusion
  12.3 2.3 stack.2
  14.6 11.5 %all-to-all-start = ((bf16[64,512,32]{1,2,0:T(8,128)(2,1)}), bf16[64,512,32]{1,2,0:T(8,128)(2,1)S(1)}, u32[]{:S(2)}, u32[]{:S(2)}) async-start(bf16[64,512,32]{1,2,0:T(8,128)(2,1)} %stack.2), calls=%async_computation | async-start | bytes 4194304 | tf_op jit(solution)/shard_map/all_to_all | solution.py:14
  26.1 0.1 fusion.119
  26.2 0.1 copy.61
  26.3 0.2 reduce_window_sum.11
  26.5 0.1 copy.62
  26.6 0.1 fusion.107
  26.7 84.1 %all-gather.3.cloned.1.call-done = bf16[2048,2056]{1,0:T(8,128)(2,1)} async-done(((bf16[32,2056]{1,0:T(8,128)(2,1)}), bf16[2048,2056]{1,0:T(8,128)(2,1)}) %all-gather.3.cloned.1.call-update) | async-done | bytes 8421392 | tf_op jit(solution)/shard_map/all_gather | solution.py:21
  110.8 1.3 fusion.94
  112.1 1.7 subtract_exponential_fusion.1
  113.8 0.1 copy.60
  113.9 2.0 fusion.58
  116.0 0.1 copy.59
  116.0 2.0 fusion.67
  118.1 2.0 fusion.70
  120.1 2.0 fusion.88
  122.2 0.1 broadcast_multiply_fusion
  122.3 3.2 %multiply_add_fusion = f32[16,4,128,128]{3,2,1,0:T(8,128)S(1)} fusion(f32[16,4,128,128]{3,2,1,0:T(8,128)} %param.32, f32[16,4,128]{2,1,0:T(4,128)S(1)} %mul.168, f32[16,4,128]{2,1,0:T(4,128)S(1)} %broadcast_multiply_fusion, f32[16,4]{1,0:T(8,128)S(1)} %copy.59), kind=kLoop, calls=%fused_computation.12 | loop fusion | flops 3145728 | bytes 8454400 | tf_op jit(solution)/shard_map/add | solution.py:79
  125.5 2.0 copy-done
  127.5 1.2 fusion.149
  128.7 0.1 multiply_reduce_fusion.1
  128.8 0.1 multiply_convert_fusion.1
  128.9 0.6 convolution_convert_fusion.1
  129.6 3.8 %all_to_all.30 = bf16[2,16,2048]{2,1,0:T(8,128)(2,1)S(1)} all-to-all(bf16[2,16,2048]{2,1,0:T(8,128)(2,1)S(1)} %broadcast_in_dim.10), channel_id=1, replica_groups=mesh['ep'=64,'tp'=2] {'tp'}, dimensions={0} | all-to-all | bytes 262144 | tf_op jit(solution)/shard_map/all_to_all | solution.py:27
  133.4 0.1 multiply_reduce_fusion
  133.6 0.1 multiply_convert_fusion
  133.7 0.4 convolution_convert_fusion
  134.1 0.5 copy.63
  134.6 26.4 %all_to_all.31 = bf16[64,2,2048]{2,1,0:T(2,128)(2,1)S(1)} all-to-all(bf16[64,2,2048]{2,1,0:T(2,128)(2,1)S(1)} %copy.63), channel_id=1, replica_groups=mesh['ep'=64,'tp'=2] {'ep'}, dimensions={0} | all-to-all | bytes 1048576 | tf_op jit(solution)/shard_map/all_to_all | solution.py:180
  161.0 0.2 reshape.107
  161.2 3.0 %fusion.37 = f32[128,1024]{1,0:T(8,128)S(1)} fusion(bf16[128,2048]{1,0:T(8,128)(2,1)S(1)} %reshape.107, bf16[1,2048,1024]{2,1,0:T(8,128)(2,1)} %param.39), kind=kOutput, calls=%fused_computation.28 | convolution fusion | flops 537001984 | bytes 5242880 | tf_op jit(solution)/shard_map/dot_general | solution.py:93
  164.2 5.0 %fusion.12 = bf16[128,2048]{1,0:T(8,128)(2,1)S(1)} fusion(bf16[1,1024,2048]{2,1,0:T(8,128)(2,1)} %param.41, f32[128,1024]{1,0:T(8,128)S(1)} %fusion.37, bf16[128,2048]{1,0:T(8,128)(2,1)S(1)} %reshape.107, bf16[1,2048,1024]{2,1,0:T(8,128)(2,1)} %param.40), kind=kOutput, calls=%fused_computation.13 | convolution fusion | flops 1075183616 | bytes 9961472 | tf_op jit(solution)/shard_map/dot_general | solution.py:96
  169.3 4.2 %all_to_all.32 = bf16[2,128,1024]{2,1,0:T(8,128)(2,1)S(1)} all-to-all(bf16[2,128,1024]{2,1,0:T(8,128)(2,1)S(1)} %bitcast.71), channel_id=1, replica_groups=mesh['ep'=64,'tp'=2] {'tp'}, dimensions={0} | all-to-all | bytes 1048576 | tf_op jit(solution)/shard_map/all_to_all | solution.py:44
  173.4 0.1 reduce_sum.71
  173.5 0.8 convert_element_type.114
  174.4 74.0 %all-gather.5.cloned.1.call-done = bf16[2048,6144]{1,0:T(8,128)(2,1)} async-done(((bf16[32,6144]{1,0:T(8,128)(2,1)}), bf16[2048,6144]{1,0:T(8,128)(2,1)}) %all-gather.5.cloned.1.call-update) | async-done | bytes 25165840 | tf_op jit(solution)/shard_map/all_gather | solution.py:21
  248.4 5.6 %fusion.4 = f32[16,2048]{1,0:T(8,128)S(1)} fusion(bf16[16,2048]{1,0:T(8,128)(2,1)S(1)} %multiply_convert_fusion, bf16[2048,6144]{1,0:T(8,128)(2,1)} %all-gather.5.cloned.1.call-done), kind=kOutput, calls=%fused_computation.4 | convolution fusion | flops 134217728 | bytes 8585216 | tf_op jit(solution)/shard_map/td,fd->tf/dot_general | solution.py:195
  254.0 9.2 %fusion.21 = bf16[16,2048]{1,0:T(8,128)(2,1)S(1)} fusion(bf16[2048,6144]{1,0:T(8,128)(2,1)} %all-gather.5.cloned.1.call-done, bf16[16,2048]{1,0:T(8,128)(2,1)S(1)} %multiply_convert_fusion, f32[16,2048]{1,0:T(8,128)S(1)} %fusion.4), kind=kOutput, calls=%fused_computation.17 | convolution fusion | flops 268664832 | bytes 17039360 | tf_op jit(solution)/shard_map/dot_general | solution.py:200
  263.2 3.8 %all_to_all.33 = bf16[2,16,1024]{2,1,0:T(8,128)(2,1)S(1)} all-to-all(bf16[2,16,1024]{2,1,0:T(8,128)(2,1)S(1)} %bitcast.75), channel_id=1, replica_groups=mesh['ep'=64,'tp'=2] {'tp'}, dimensions={0} | all-to-all | bytes 131072 | tf_op jit(solution)/shard_map/all_to_all | solution.py:44
  267.0 8.6 %all-to-all-start.4 = ((bf16[64,2,1024]{2,1,0:T(2,128)(2,1)}), bf16[64,2,1024]{2,1,0:T(2,128)(2,1)S(1)}, u32[]{:S(2)}, u32[]{:S(2)}) async-start(bf16[64,2,1024]{2,1,0:T(2,128)(2,1)} %convert_element_type.114), calls=%async_computation.4 | async-start | bytes 524288 | tf_op jit(solution)/shard_map/all_to_all | solution.py:186
  275.6 0.1 select_reduce_fusion
  275.8 10.8 %all-to-all-done.4 = bf16[64,2,1024]{2,1,0:T(2,128)(2,1)S(1)} async-done(((bf16[64,2,1024]{2,1,0:T(2,128)(2,1)}), bf16[64,2,1024]{2,1,0:T(2,128)(2,1)S(1)}, u32[]{:S(2)}, u32[]{:S(2)}) %all-to-all-start.4) | async-done | bytes 262176 | tf_op jit(solution)/shard_map/all_to_all | solution.py:186
  286.5 0.9 fusion.54
  (42 shorter events, 0.3 us)
Async XLA Ops:
  7.2 19.0 %copy-start.3 = (s32[16,4]{0,1:T(4,128)S(1)}, s32[16,4]{0,1:T(4,128)}, u32[]{:S(2)}) copy-start(s32[16,4]{0,1:T(4,128)} %param.37) | copy-start | bytes 772
  7.2 19.4 %copy-start.1 = (bf16[16,2048]{1,0:T(8,128)(2,1)S(1)}, bf16[16,2048]{1,0:T(8,128)(2,1)}, u32[]{:S(2)}) copy-start(bf16[16,2048]{1,0:T(8,128)(2,1)} %param.23) | copy-start | bytes 196612
  7.2 103.7 %copy-start.8 = (f32[2048]{0:T(1024)S(1)}, f32[2048]{0:T(1024)}, u32[]{:S(2)}) copy-start(f32[2048]{0:T(1024)} %param.24) | copy-start | bytes 24580
  7.2 103.6 %all-gather.3.cloned.1.call-start = ((), (), s32[]{:S(2)}) async-start(), calls=%async_computation.6 | async-start | bytes 9052160 | tf_op jit(solution)/shard_map/all_gather | solution.py:21
  10.4 101.8 %copy-start.9 = (f32[16,4]{0,1:T(4,128)S(1)}, f32[16,4]{0,1:T(4,128)}, u32[]{:S(2)}) copy-start(f32[16,4]{0,1:T(4,128)} %param.33) | copy-start | bytes 772
  10.4 101.8 %copy-start.10 = (f32[4]{0:T(128)S(1)}, f32[4]{0:T(128)}, u32[]{:S(2)}) copy-start(f32[4]{0:T(128)} %param.31) | copy-start | bytes 52
  10.4 238.0 %all-gather.5.cloned.1.call-start = ((), (), s32[]{:S(2)}) async-start(), calls=%async_computation.7 | async-start | bytes 25559040 | tf_op jit(solution)/shard_map/all_gather | solution.py:21
  14.6 114.3 %all-to-all-start = ((bf16[64,512,32]{1,2,0:T(8,128)(2,1)}), bf16[64,512,32]{1,2,0:T(8,128)(2,1)S(1)}, u32[]{:S(2)}, u32[]{:S(2)}) async-start(bf16[64,512,32]{1,2,0:T(8,128)(2,1)} %stack.2), calls=%async_computation | async-start | bytes 4194304 | tf_op jit(solution)/shard_map/all_to_all | solution.py:14
  113.8 8.3 %copy-start.5 = (f32[16,4]{0,1:T(4,128)}, f32[16,4]{0,1:T(4,128)S(1)}, u32[]{:S(2)}) copy-start(f32[16,4]{0,1:T(4,128)S(1)} %get-tuple-element.6) | copy-start | bytes 772
  125.5 2.0 copy-start
  127.5 1.3 copy-start.4
  127.5 6.1 %copy-start.2 = (f32[2048]{0:T(1024)S(1)}, f32[2048]{0:T(1024)}, u32[]{:S(2)}) copy-start(f32[2048]{0:T(1024)} %param.36) | copy-start | bytes 24580
  254.0 21.6 %copy-start.6 = (f32[2048]{0:T(1024)S(1)}, f32[2048]{0:T(1024)}, u32[]{:S(2)}) copy-start(f32[2048]{0:T(1024)} %param.45) | copy-start | bytes 24580
  254.0 21.6 %copy-start.7 = (f32[16,4]{0,1:T(4,128)S(1)}, f32[16,4]{0,1:T(4,128)}, u32[]{:S(2)}) copy-start(f32[16,4]{0,1:T(4,128)} %param.38) | copy-start | bytes 772
  267.0 19.5 %all-to-all-start.4 = ((bf16[64,2,1024]{2,1,0:T(2,128)(2,1)}), bf16[64,2,1024]{2,1,0:T(2,128)(2,1)S(1)}, u32[]{:S(2)}, u32[]{:S(2)}) async-start(bf16[64,2,1024]{2,1,0:T(2,128)(2,1)} %convert_element_type.114), calls=%async_computation.4 | async-start | bytes 524288 | tf_op jit(solution)/shard_map/all_to_all | solution.py:186
Sparse Core Ops, SparseCore 0:
  11.4 99.4 all-gather.2
  113.6 134.7 all-gather.4
